TPU v7x, 32 devices: a whole 2x2x4 slice. The times are simulated.
32 devices in a mesh: grp: 2 (over y), sp: 4 (over z), tp: 4 (over x, core).
Axes of the slice: x: 2, y: 2, z: 4, core: 2. Of those that a mesh axis runs over, the one named last changes fastest.
Arguments:
- queries: bfloat16 [6144, 1024], P(('grp', 'sp'), 'tp'), parts along dimension 0, may hold values from -160 to 160
- key_rows: bfloat16 [6144, 256], P(('grp', 'sp'), 'tp'), parts along dimension 0, may hold values from -4 to 4
- value_rows: bfloat16 [6144, 256], P(('grp', 'sp'), 'tp'), parts along dimension 0, may hold values from -5 to 5
- sink_logits: float32 [16], P('tp'), may hold values from 2 to 6
- out_weight: bfloat16 [1024, 2048], replicated, may hold values from -0.75 to 0.75
- residual: bfloat16 [6144, 2048], P(('grp', 'sp', 'tp')), parts along dimension 0, may hold values from -6 to 6
- norm_gain: float32 [2048], replicated, may hold values from 0.1 to 1.9
- up_weight: bfloat16 [2048, 4096], P('sp', 'tp'), may hold values from -0.125 to 0.125
- down_weight: bfloat16 [4096, 2048], P('tp', 'sp'), may hold values from -0.09375 to 0.09375
Outputs:
- layer_out: bfloat16 [6144, 2048], P(('grp', 'sp', 'tp')), parts along dimension 0
There are 2 independent parts, one for each index of `grp`. A program takes and returns all parts, laid end to end along the dimension named above; an argument that names none is the same for every part. Nothing has to cross between parts.
All inputs are finite; a program needn't handle non-finite values.
Results may differ from a plain program's by a relative error of at most 0.017.
Values may be sent and summed in bfloat16 or wider, within the bound.
A program may use at most 64 MiB of HBM per device.

v0:
```python
import jax
import jax.numpy as jnp
from jax import lax
from jax.sharding import PartitionSpec as P

HEAD_DIM = 64
WINDOW = 128


def shifted(value, axis, steps):
    count = lax.axis_size(axis)
    leading, last = (max(0, -steps), min(count, count - steps))
    return lax.ppermute(value, axis, [(source, source + steps) for source in range(leading, last)])


def band_attend(queries, key_rows, value_rows, sink_logits, tail_keys, tail_values, offset):
    rows = queries.shape[0]
    kv_heads = key_rows.shape[1] // HEAD_DIM
    group = queries.shape[1] // (kv_heads * HEAD_DIM)
    blocks = rows // WINDOW
    all_keys = jnp.concatenate([tail_keys, key_rows], axis=0).reshape(
        blocks + 1, WINDOW, kv_heads, HEAD_DIM
    )
    all_values = jnp.concatenate([tail_values, value_rows], axis=0).reshape(
        blocks + 1, WINDOW, kv_heads, HEAD_DIM
    )
    key_blocks = jnp.concatenate([all_keys[:-1], all_keys[1:]], axis=1)
    value_blocks = jnp.concatenate([all_values[:-1], all_values[1:]], axis=1)
    query_blocks = queries.reshape(blocks, WINDOW, kv_heads, group, HEAD_DIM)
    scores = jnp.einsum(
        "nqkgd,nskd->nkgqs", query_blocks, key_blocks, preferred_element_type=jnp.float32
    ) * HEAD_DIM ** (-0.5)
    q_local = jnp.arange(WINDOW, dtype=jnp.int32) + WINDOW
    k_local = jnp.arange(2 * WINDOW, dtype=jnp.int32)
    distance = q_local[:, None] - k_local[None, :]
    key_position = (
        offset + (jnp.arange(blocks, dtype=jnp.int32)[:, None] - 1) * WINDOW + k_local[None, :]
    )
    valid = ((distance >= 0) & (distance < WINDOW))[None] & (key_position >= 0)[:, None, :]
    scores = jnp.where(valid[:, None, None], scores, -1e30)
    sink = sink_logits.reshape(kv_heads, group)[None, :, :, None, None]
    top = jnp.maximum(jnp.max(scores, axis=-1, keepdims=True), sink)
    weights = jnp.exp(scores - top)
    total = jnp.sum(weights, axis=-1, keepdims=True) + jnp.exp(sink - top)
    probs = (weights / total).astype(jnp.bfloat16)
    result = jnp.einsum(
        "nkgqs,nskd->nqkgd", probs, value_blocks, preferred_element_type=jnp.float32
    )
    return result.astype(jnp.bfloat16).reshape(rows, kv_heads * group * HEAD_DIM)


def body(
    queries,
    key_rows,
    value_rows,
    sink_logits,
    out_weight,
    residual,
    norm_gain,
    up_weight,
    down_weight,
):
    rows = queries.shape[0]
    width = key_rows.shape[1]
    kv_pair = jnp.concatenate([key_rows[rows - WINDOW :], value_rows[rows - WINDOW :]], axis=1)
    tail = shifted(kv_pair, "sp", 1)
    offset = lax.axis_index("sp") * rows
    attended = band_attend(
        queries, key_rows, value_rows, sink_logits, tail[:, :width], tail[:, width:], offset
    )
    head_cols = attended.shape[1]
    own_rows = lax.dynamic_slice_in_dim(out_weight, lax.axis_index("tp") * head_cols, head_cols, 0)
    projected = lax.psum_scatter(
        jnp.dot(attended, own_rows, preferred_element_type=jnp.float32).astype(jnp.bfloat16),
        "tp",
        scatter_dimension=0,
        tiled=True,
    ).astype(jnp.float32)
    mixed32 = (residual.astype(jnp.float32) + projected).astype(jnp.bfloat16).astype(jnp.float32)
    scale = lax.rsqrt(jnp.mean(mixed32 * mixed32, axis=-1, keepdims=True) + 1e-06)
    normed = (mixed32 * scale * norm_gain).astype(jnp.bfloat16)
    all_rows = lax.all_gather(normed, "tp", axis=0, tiled=True)
    before = jnp.dot(
        all_rows,
        lax.all_gather(up_weight, "sp", axis=0, tiled=True),
        preferred_element_type=jnp.float32,
    )
    hidden = jnp.square(jax.nn.relu(before)).astype(jnp.bfloat16)
    terms = jnp.dot(
        hidden,
        lax.all_gather(down_weight, "sp", axis=1, tiled=True),
        preferred_element_type=jnp.float32,
    )
    down = lax.psum_scatter(
        terms.astype(jnp.bfloat16), "tp", scatter_dimension=0, tiled=True
    ).astype(jnp.float32)
    return (mixed32 + down).astype(jnp.bfloat16)


def solution(mesh):
    in_specs = (
        P(("grp", "sp"), "tp"),
        P(("grp", "sp"), "tp"),
        P(("grp", "sp"), "tp"),
        P("tp"),
        P(),
        P(("grp", "sp", "tp"), None),
        P(),
        P("sp", "tp"),
        P("tp", "sp"),
    )
    out_specs = P(("grp", "sp", "tp"), None)
    return jax.shard_map(body, mesh=mesh, in_specs=in_specs, out_specs=out_specs, check_vma=False)
```

profile of v0, /device:TPU:0, one launch (start us, length us, event | category | flops | bytes accessed | tf_op | source)
XLA Modules:
  0.0 278.1 jit_solution(6048597584942686161)
XLA Ops:
  7.4 0.0 reduce-scatter.3.cloned.1.call-start
  7.4 0.7 slice.32
  8.1 0.7 slice.33
  8.8 4.9 %collective-permute-start = (bf16[128,128]{0,1:T(8,128)(2,1)S(1)}, bf16[128,128]{0,1:T(8,128)(2,1)S(1)}, u32[]{:S(2)}, u32[]{:S(2)}) collective-permute-start(bf16[128,128]{0,1:T(8,128)(2,1)S(1)} %pad_maximum_fusion.2), channel_id=1, source_target_pairs={{0,4},{4,8},{8,12},{1,5},{5,9},{9,13},{2,6},{6,10},{10,14},{3,7},{... | collective-permute-start | bytes 98312 | tf_op jit(solution)/shard_map/ppermute | solution.py:13
  13.8 0.1 add_compare_fusion
  13.9 0.3 broadcast_and_fusion
  14.2 1.0 slice.41
  15.2 1.0 slice.37
  16.3 1.8 reshape.128
  18.1 0.0 copy-start.3
  18.2 0.0 collective-permute-done
  18.2 0.9 pad_maximum_fusion
  19.1 0.1 slice.40
  19.3 0.1 slice.36
  19.5 0.7 fusion.1
  20.2 0.0 copy-done.3
  20.2 0.1 broadcast_maximum_fusion
  20.3 0.7 fusion
  21.0 0.1 exponential_add_fusion
  21.1 0.9 fusion.12
  22.0 0.3 copy.19
  22.3 4.0 %convolution_convert_fusion.1 = bf16[768,2048]{1,0:T(8,128)(2,1)} fusion(bf16[1024,2048]{1,0:T(8,128)(2,1)} %param.13, s32[]{:T(128)S(6)} %select_n.8, bf16[32,8,6,128]{3,2,1,0:T(8,128)(2,1)S(1)} %bitcast.60), kind=kOutput, calls=%fused_computation.1 | convolution fusion | flops 806879232 | bytes 4587524 | tf_op jit(solution)/shard_map/dot_general | solution.py:74
  26.3 0.0 copy-start
  26.3 0.0 copy-start.2
  26.3 0.0 reduce-scatter.3.cloned.1.call-update
  26.3 0.0 all-gather.6.cloned.1.call-start
  26.4 0.5 all-gather.6.cloned.1.call-update
  26.9 0.0 all-gather.8.cloned.1.call-start
  27.0 0.5 all-gather.8.cloned.1.call-update
  27.5 0.0 all-gather.4.cloned.1.call-start
  27.5 37.0 %reduce-scatter.3.cloned.1.call-done = bf16[192,2048]{1,0:T(8,128)(2,1)} async-done(((bf16[768,2048]{1,0:T(8,128)(2,1)}), bf16[192,2048]{1,0:T(8,128)(2,1)}) %reduce-scatter.3.cloned.1.call-update) | async-done | bytes 786448 | tf_op jit(solution)/shard_map/reduce_scatter | solution.py:73
  64.6 0.0 copy-done
  64.6 1.5 fusion.2
  66.1 0.0 copy-done.2
  66.1 2.3 fusion.4
  68.4 0.0 all-gather.4.cloned.1.call-update
  68.4 0.0 reduce-scatter.5.cloned.1.call-start
  68.5 40.8 %all-gather.6.cloned.1.call-done = bf16[2048,1024]{1,0:T(8,128)(2,1)} async-done(((bf16[512,1024]{1,0:T(8,128)(2,1)}), bf16[2048,1024]{1,0:T(8,128)(2,1)}) %all-gather.6.cloned.1.call-update) | async-done | bytes 4194320 | tf_op jit(solution)/shard_map/all_gather | solution.py:85
  109.2 80.6 %all-gather.8.cloned.1.call-done = bf16[1024,2048]{1,0:T(8,128)(2,1)} async-done(((bf16[1024,512]{1,0:T(8,128)(2,1)}), bf16[1024,2048]{1,0:T(8,128)(2,1)}) %all-gather.8.cloned.1.call-update) | async-done | bytes 4194320 | tf_op jit(solution)/shard_map/all_gather | solution.py:91
  189.8 28.3 %all-gather.4.cloned.1.call-done = bf16[768,2048]{1,0:T(8,128)(2,1)} async-done(((bf16[192,2048]{1,0:T(8,128)(2,1)}), bf16[768,2048]{1,0:T(8,128)(2,1)}) %all-gather.4.cloned.1.call-update) | async-done | bytes 3145744 | tf_op jit(solution)/shard_map/all_gather | solution.py:82
  218.1 11.9 %convolution_convert_fusion = bf16[768,2048]{1,0:T(8,128)(2,1)} fusion(bf16[1024,2048]{1,0:T(8,128)(2,1)} %all-gather.8.cloned.1.call-done, bf16[768,2048]{1,0:T(8,128)(2,1)} %all-gather.4.cloned.1.call-done, bf16[2048,1024]{1,0:T(8,128)(2,1)} %all-gather.6.cloned.1.call-done), kind=kOutput, calls=%fused_computation | convolution fusion | flops 6446383104 | bytes 14680064 | tf_op jit(solution)/shard_map/dot_general | solution.py:89
  230.0 0.0 copy-start.1
  230.0 0.0 reduce-scatter.5.cloned.1.call-update
  230.0 38.0 %reduce-scatter.5.cloned.1.call-done = bf16[192,2048]{1,0:T(8,128)(2,1)} async-done(((bf16[768,2048]{1,0:T(8,128)(2,1)}), bf16[192,2048]{1,0:T(8,128)(2,1)}) %reduce-scatter.5.cloned.1.call-update) | async-done | bytes 786448 | tf_op jit(solution)/shard_map/reduce_scatter | solution.py:94
  268.1 0.0 copy-done.1
  268.1 2.4 fusion.5
  (10 shorter events, 0.1 us)
Async XLA Ops:
  7.4 57.2 %reduce-scatter.3.cloned.1.call-start = ((), (), s32[]{:S(2)}) async-start(), calls=%async_computation.2 | async-start | bytes 3932160 | tf_op jit(solution)/shard_map/reduce_scatter | solution.py:73
  8.8 9.3 %collective-permute-start = (bf16[128,128]{0,1:T(8,128)(2,1)S(1)}, bf16[128,128]{0,1:T(8,128)(2,1)S(1)}, u32[]{:S(2)}, u32[]{:S(2)}) collective-permute-start(bf16[128,128]{0,1:T(8,128)(2,1)S(1)} %pad_maximum_fusion.2), channel_id=1, source_target_pairs={{0,4},{4,8},{8,12},{1,5},{5,9},{9,13},{2,6},{6,10},{10,14},{3,7},{... | collective-permute-start | bytes 98312 | tf_op jit(solution)/shard_map/ppermute | solution.py:13
  18.1 2.0 copy-start.3
  26.3 38.3 %copy-start = (bf16[192,2048]{1,0:T(8,128)(2,1)S(1)}, bf16[192,2048]{1,0:T(8,128)(2,1)}, u32[]{:S(2)}) copy-start(bf16[192,2048]{1,0:T(8,128)(2,1)} %param.14) | copy-start | bytes 2359300
  26.3 39.8 %copy-start.2 = (f32[2048]{0:T(1024)S(1)}, f32[2048]{0:T(1024)}, u32[]{:S(2)}) copy-start(f32[2048]{0:T(1024)} %param.15) | copy-start | bytes 24580
  26.3 82.9 %all-gather.6.cloned.1.call-start = ((), (), s32[]{:S(2)}) async-start(), calls=%async_computation.4 | async-start | bytes 5242880 | tf_op jit(solution)/shard_map/all_gather | solution.py:85
  26.9 162.9 %all-gather.8.cloned.1.call-start = ((), (), s32[]{:S(2)}) async-start(), calls=%async_computation.5 | async-start | bytes 5242880 | tf_op jit(solution)/shard_map/all_gather | solution.py:91
  27.5 190.6 %all-gather.4.cloned.1.call-start = ((), (), s32[]{:S(2)}) async-start(), calls=%async_computation.3 | async-start | bytes 3932160 | tf_op jit(solution)/shard_map/all_gather | solution.py:82
  68.4 199.7 %reduce-scatter.5.cloned.1.call-start = ((), (), s32[]{:S(2)}) async-start(), calls=%async_computation.6 | async-start | bytes 3932160 | tf_op jit(solution)/shard_map/reduce_scatter | solution.py:94
  230.0 38.1 %copy-start.1 = (bf16[192,2048]{1,0:T(8,128)(2,1)S(1)}, bf16[192,2048]{1,0:T(8,128)(2,1)}, u32[]{:S(2)}) copy-start(bf16[192,2048]{1,0:T(8,128)(2,1)} %reduce-scatter.3.cloned.1.call-done) | copy-start | bytes 2359300
Sparse Core Ops, SparseCore 0:
  26.4 38.0 reduce-scatter.2
  230.2 37.8 reduce-scatter.4
Sparse Core Ops, SparseCore 1:
  28.4 80.8 all-gather.5
  110.7 79.1 all-gather.7
  191.2 26.8 all-gather.3
where the time goes:
time: 279 us; the launch traced here: 278 us
  waiting for transfers between devices  226 us (81%)
  matrix products  17.5 us (6%)
  between operations  15.2 us (5%)
  other arithmetic  8.43 us (3%)
  local copies, waits for them, and re-layouts  5.95 us (2%)
  starting transfers between devices  5.11 us (2%)
    all_gather x1, waiting for transfers between devices, body(): lax.all_gather(down_weight, 'sp', axis=1, tiled=True)  80.6 us
    all_gather x1, waiting for transfers between devices, body(): lax.all_gather(up_weight, 'sp', axis=0, tiled=True)  40.8 us
    reduce_scatter x1, waiting for transfers between devices, body(): lax.psum_scatter(terms.astype(jnp.bfloat16), 'tp', scatter_dimension=0, t...  38 us
    reduce_scatter x1, waiting for transfers between devices, body(): lax.psum_scatter(jnp.dot(attended, own_rows, preferred_element_type=jnp.f...  37 us
    all_gather x1, waiting for transfers between devices, body(): all_rows = lax.all_gather(normed, 'tp', axis=0, tiled=True)  28.3 us
    dot_general x1, matrix products, body(): jnp.dot(hidden, lax.all_gather(down_weight, 'sp', axis=1, tiled=True), pr...  11.9 us
  transfers between devices with their start and end apart: 6, of which 5 were waited for; matrix products, arithmetic and copies ran while one was open for 3% of the time, Pallas kernels for 0%

commit v1 on v0

--- a/solution.py
+++ b/solution.py
@@ -79,7 +79,12 @@
     mixed32 = (residual.astype(jnp.float32) + projected).astype(jnp.bfloat16).astype(jnp.float32)
     scale = lax.rsqrt(jnp.mean(mixed32 * mixed32, axis=-1, keepdims=True) + 1e-06)
     normed = (mixed32 * scale * norm_gain).astype(jnp.bfloat16)
-    all_rows = lax.all_gather(normed, "tp", axis=0, tiled=True)
+    ring = [normed]
+    for hop in range(3):
+        ring.append(lax.ppermute(ring[-1], "tp", [(dev, (dev + 1) % 4) for dev in range(4)]))
+    all_rows = jnp.roll(
+        jnp.concatenate(ring[::-1], axis=0), (lax.axis_index("tp") + 1) * ring[0].shape[0], axis=0
+    )
     before = jnp.dot(
         all_rows,
         lax.all_gather(up_weight, "sp", axis=0, tiled=True),

time: 279 us -> 253 us (0.907)
  waiting for transfers between devices: 226 us -> 187 us
  local copies, waits for them, and re-layouts: 5.95 us -> 18.1 us
    all_gather x1, waiting for transfers between devices: 40.8 us -> 0.01 us  [body(): lax.all_gather(up_weight, 'sp', axis=0, tiled=True)]
    ppermute x0 -> x3, waiting for transfers between devices: none -> 34.3 us  [body(): lax.ppermute(ring[-1], 'tp', [(dev, (dev + 1) % 4) for dev in range(4)])]
    all_gather x1 -> x0, waiting for transfers between devices: 28.3 us -> none  [body(): all_rows = lax.all_gather(normed, 'tp', axis=0, tiled=True)]
    unnamed x8 -> x15, local copies, waits for them, and re-layouts: 0.02 us -> 8.97 us
  transfers between devices with their start and end apart: 6 -> 8, of which waited for: 5 -> 6; matrix products, arithmetic and copies ran while one was open for 3% -> 7% of each run, Pallas kernels for 0% -> 0%
where the time goes in v1:
time: 253 us
  waiting for transfers between devices  187 us (74%)
  matrix products  19.5 us (8%)
  local copies, waits for them, and re-layouts  18.1 us (7%)
  between operations  15 us (6%)
  other arithmetic  8.19 us (3%)
  starting transfers between devices  5.14 us (2%)
    all_gather x1, waiting for transfers between devices, body(): lax.all_gather(down_weight, 'sp', axis=1, tiled=True)  77.9 us
    reduce_scatter x1, waiting for transfers between devices, body(): lax.psum_scatter(jnp.dot(attended, own_rows, preferred_element_type=jnp.f...  37 us
    reduce_scatter x1, waiting for transfers between devices, body(): lax.psum_scatter(terms.astype(jnp.bfloat16), 'tp', scatter_dimension=0, t...  36.5 us
    ppermute x3, waiting for transfers between devices, body(): lax.ppermute(ring[-1], 'tp', [(dev, (dev + 1) % 4) for dev in range(4)])  34.3 us
    dot_general x1, matrix products, body(): jnp.dot(hidden, lax.all_gather(down_weight, 'sp', axis=1, tiled=True), pr...  11.9 us
    unnamed x15, local copies, waits for them, and re-layouts  8.97 us
  transfers between devices with their start and end apart: 8, of which 6 were waited for; matrix products, arithmetic and copies ran while one was open for 7% of the time, Pallas kernels for 0%

profile of v1, /device:TPU:0, one launch (start us, length us, event | category | flops | bytes accessed | tf_op | source)
XLA Modules:
  0.0 252.8 jit_solution(9443562196966784608)
XLA Ops:
  7.4 0.0 reduce-scatter.3.cloned.1.call-start
  7.4 0.7 slice.32
  8.1 0.7 slice.33
  8.8 4.9 %collective-permute-start = (bf16[128,128]{0,1:T(8,128)(2,1)S(1)}, bf16[128,128]{0,1:T(8,128)(2,1)S(1)}, u32[]{:S(2)}, u32[]{:S(2)}) collective-permute-start(bf16[128,128]{0,1:T(8,128)(2,1)S(1)} %pad_maximum_fusion.2), channel_id=1, source_target_pairs={{0,4},{4,8},{8,12},{1,5},{5,9},{9,13},{2,6},{6,10},{10,14},{3,7},{... | collective-permute-start | bytes 98312 | tf_op jit(solution)/shard_map/ppermute | solution.py:13
  13.8 0.1 add_compare_fusion
  13.9 0.3 broadcast_and_fusion
  14.2 1.0 slice.41
  15.2 1.0 slice.37
  16.3 2.5 %reshape.128 = bf16[6,128,4,64]{3,2,1,0:T(4,128)(2,1)} reshape(bf16[768,256]{1,0:T(8,128)(2,1)} %param.9) | data formatting | bytes 786432 | tf_op jit(solution)/shard_map/reshape.10
  18.8 0.0 copy-start.3
  18.8 0.6 copy.13
  19.5 0.0 collective-permute-done
  19.5 1.6 pad_maximum_fusion
  21.0 0.1 slice.40
  21.2 1.9 fusion.3
  23.1 0.0 copy-done.3
  23.1 0.1 broadcast_maximum_fusion
  23.1 0.7 fusion.2
  23.8 0.1 exponential_add_fusion
  23.9 1.0 slice.36
  25.0 1.8 fusion.16
  26.8 0.3 copy.19
  27.1 3.9 %convolution_convert_fusion.1 = bf16[768,2048]{1,0:T(8,128)(2,1)} fusion(bf16[1024,2048]{1,0:T(8,128)(2,1)} %param.13, s32[]{:T(128)S(6)} %select_n.21, bf16[32,8,6,128]{3,2,1,0:T(8,128)(2,1)S(1)} %bitcast.59), kind=kOutput, calls=%fused_computation.1 | convolution fusion | flops 806879232 | bytes 4587524 | tf_op jit(solution)/shard_map/dot_general | solution.py:74
  31.0 0.0 copy-start
  31.0 0.0 copy-start.2
  31.0 0.0 reduce-scatter.3.cloned.1.call-update
  31.0 0.0 all-gather.3.cloned.1.call-start
  31.1 0.5 all-gather.3.cloned.1.call-update
  31.6 0.0 all-gather.5.cloned.1.call-start
  31.6 0.5 all-gather.5.cloned.1.call-update
  32.2 0.0 reduce-scatter.5.cloned.1.call-start
  32.2 37.0 %reduce-scatter.3.cloned.1.call-done = bf16[192,2048]{1,0:T(8,128)(2,1)} async-done(((bf16[768,2048]{1,0:T(8,128)(2,1)}), bf16[192,2048]{1,0:T(8,128)(2,1)}) %reduce-scatter.3.cloned.1.call-update) | async-done | bytes 786448 | tf_op jit(solution)/shard_map/reduce_scatter | solution.py:73
  69.3 0.0 copy-done
  69.3 1.5 fusion.6
  70.7 0.0 copy-done.2
  70.7 1.5 fusion.8
  72.2 0.1 collective-permute-start.1
  72.3 11.4 %collective-permute-done.1 = bf16[192,2048]{1,0:T(8,128)(2,1)S(1)} collective-permute-done((bf16[192,2048]{1,0:T(8,128)(2,1)S(1)}, bf16[192,2048]{1,0:T(8,128)(2,1)S(1)}, u32[]{:S(2)}, u32[]{:S(2)}) %collective-permute-start.1) | collective-permute-done | bytes 786464 | tf_op jit(solution)/shard_map/ppermute | solution.py:84
  83.7 0.0 collective-permute-start.2
  83.7 11.4 %collective-permute-done.2 = bf16[192,2048]{1,0:T(8,128)(2,1)S(1)} collective-permute-done((bf16[192,2048]{1,0:T(8,128)(2,1)S(1)}, bf16[192,2048]{1,0:T(8,128)(2,1)S(1)}, u32[]{:S(2)}, u32[]{:S(2)}) %collective-permute-start.2) | collective-permute-done | bytes 786464 | tf_op jit(solution)/shard_map/ppermute | solution.py:84
  95.1 0.0 collective-permute-start.3
  95.1 11.5 %collective-permute-done.3 = bf16[192,2048]{1,0:T(8,128)(2,1)} collective-permute-done((bf16[192,2048]{1,0:T(8,128)(2,1)S(1)}, bf16[192,2048]{1,0:T(8,128)(2,1)}, u32[]{:S(2)}, u32[]{:S(2)}) %collective-permute-start.3) | collective-permute-done | bytes 786464 | tf_op jit(solution)/shard_map/ppermute | solution.py:84
  106.6 2.1 constant_dynamic-update-slice_fusion.7
  108.7 1.0 constant_dynamic-update-slice_fusion.6
  109.7 0.9 constant_dynamic-update-slice_fusion.5
  110.6 0.9 constant_dynamic-update-slice_fusion.4
  111.6 2.1 constant_dynamic-update-slice_fusion.3
  113.7 1.0 constant_dynamic-update-slice_fusion.2
  114.6 1.0 constant_dynamic-update-slice_fusion.1
  115.6 0.9 constant_dynamic-update-slice_fusion
  116.5 0.0 all-gather.3.cloned.1.call-done
  116.5 77.9 %all-gather.5.cloned.1.call-done = bf16[1024,2048]{1,0:T(8,128)(2,1)} async-done(((bf16[1024,512]{1,0:T(8,128)(2,1)}), bf16[1024,2048]{1,0:T(8,128)(2,1)}) %all-gather.5.cloned.1.call-update) | async-done | bytes 4194320 | tf_op jit(solution)/shard_map/all_gather | solution.py:96
  194.5 11.9 %convolution_convert_fusion = bf16[768,2048]{1,0:T(8,128)(2,1)} fusion(bf16[1024,2048]{1,0:T(8,128)(2,1)} %all-gather.5.cloned.1.call-done, bf16[2048,1024]{1,0:T(8,128)(2,1)} %all-gather.3.cloned.1.call-done, bf16[1536,2048]{1,0:T(8,128)(2,1)} %constant_dynamic-update-slice_fusion, s32[]{:T(128)S(6)} %select_n.23), kind=kOutput, calls=%fused_computation | convolution fusion | flops 6446383104 | bytes 14680068 | tf_op jit(solution)/shard_map/dot_general | solution.py:94
  206.4 0.0 copy-start.1
  206.4 0.0 reduce-scatter.5.cloned.1.call-update
  206.4 36.5 %reduce-scatter.5.cloned.1.call-done = bf16[192,2048]{1,0:T(8,128)(2,1)} async-done(((bf16[768,2048]{1,0:T(8,128)(2,1)}), bf16[192,2048]{1,0:T(8,128)(2,1)}) %reduce-scatter.5.cloned.1.call-update) | async-done | bytes 786448 | tf_op jit(solution)/shard_map/reduce_scatter | solution.py:99
  242.9 0.0 copy-done.1
  242.9 2.4 fusion.9
  (9 shorter events, 0.1 us)
Async XLA Ops:
  7.4 61.9 %reduce-scatter.3.cloned.1.call-start = ((), (), s32[]{:S(2)}) async-start(), calls=%async_computation.2 | async-start | bytes 3932160 | tf_op jit(solution)/shard_map/reduce_scatter | solution.py:73
  8.8 10.6 %collective-permute-start = (bf16[128,128]{0,1:T(8,128)(2,1)S(1)}, bf16[128,128]{0,1:T(8,128)(2,1)S(1)}, u32[]{:S(2)}, u32[]{:S(2)}) collective-permute-start(bf16[128,128]{0,1:T(8,128)(2,1)S(1)} %pad_maximum_fusion.2), channel_id=1, source_target_pairs={{0,4},{4,8},{8,12},{1,5},{5,9},{9,13},{2,6},{6,10},{10,14},{3,7},{... | collective-permute-start | bytes 98312 | tf_op jit(solution)/shard_map/ppermute | solution.py:13
  18.8 4.3 %copy-start.3 = (f32[4]{0:T(128)S(1)}, f32[4]{0:T(128)}, u32[]{:S(2)}) copy-start(f32[4]{0:T(128)} %param.12) | copy-start | bytes 52
  31.0 38.3 %copy-start = (bf16[192,2048]{1,0:T(8,128)(2,1)S(1)}, bf16[192,2048]{1,0:T(8,128)(2,1)}, u32[]{:S(2)}) copy-start(bf16[192,2048]{1,0:T(8,128)(2,1)} %param.14) | copy-start | bytes 2359300
  31.0 39.7 %copy-start.2 = (f32[2048]{0:T(1024)S(1)}, f32[2048]{0:T(1024)}, u32[]{:S(2)}) copy-start(f32[2048]{0:T(1024)} %param.15) | copy-start | bytes 24580
  31.0 85.5 %all-gather.3.cloned.1.call-start = ((), (), s32[]{:S(2)}) async-start(), calls=%async_computation.3 | async-start | bytes 5242880 | tf_op jit(solution)/shard_map/all_gather | solution.py:90
  31.6 162.9 %all-gather.5.cloned.1.call-start = ((), (), s32[]{:S(2)}) async-start(), calls=%async_computation.4 | async-start | bytes 5242880 | tf_op jit(solution)/shard_map/all_gather | solution.py:96
  32.2 210.7 %reduce-scatter.5.cloned.1.call-start = ((), (), s32[]{:S(2)}) async-start(), calls=%async_computation.5 | async-start | bytes 3932160 | tf_op jit(solution)/shard_map/reduce_scatter | solution.py:99
  72.2 11.5 %collective-permute-start.1 = (bf16[192,2048]{1,0:T(8,128)(2,1)S(1)}, bf16[192,2048]{1,0:T(8,128)(2,1)S(1)}, u32[]{:S(2)}, u32[]{:S(2)}) collective-permute-start(bf16[192,2048]{1,0:T(8,128)(2,1)S(1)} %fusion.8), channel_id=1, source_target_pairs={{0,1},{1,2},{2,3},{3,0},{4,5},{5,6},{6,7},{7,4},{8,9},{9,10},{10,1... | collective-permute-start | bytes 2359304 | tf_op jit(solution)/shard_map/ppermute | solution.py:84
  83.7 11.4 %collective-permute-start.2 = (bf16[192,2048]{1,0:T(8,128)(2,1)S(1)}, bf16[192,2048]{1,0:T(8,128)(2,1)S(1)}, u32[]{:S(2)}, u32[]{:S(2)}) collective-permute-start(bf16[192,2048]{1,0:T(8,128)(2,1)S(1)} %collective-permute-done.1), channel_id=1, source_target_pairs={{0,1},{1,2},{2,3},{3,0},{4,5},{5,6},{6,7},{7,4},{8,9},{9,10},{10,1... | collective-permute-start | bytes 2359304 | tf_op jit(solution)/shard_map/ppermute | solution.py:84
  95.1 11.5 %collective-permute-start.3 = (bf16[192,2048]{1,0:T(8,128)(2,1)S(1)}, bf16[192,2048]{1,0:T(8,128)(2,1)}, u32[]{:S(2)}, u32[]{:S(2)}) collective-permute-start(bf16[192,2048]{1,0:T(8,128)(2,1)S(1)} %collective-permute-done.2), channel_id=1, source_target_pairs={{0,1},{1,2},{2,3},{3,0},{4,5},{5,6},{6,7},{7,4},{8,9},{9,10},{10,1... | collective-permute-start | bytes 2359304 | tf_op jit(solution)/shard_map/ppermute | solution.py:84
  206.4 36.6 %copy-start.1 = (bf16[192,2048]{1,0:T(8,128)(2,1)S(1)}, bf16[192,2048]{1,0:T(8,128)(2,1)}, u32[]{:S(2)}) copy-start(bf16[192,2048]{1,0:T(8,128)(2,1)} %reduce-scatter.3.cloned.1.call-done) | copy-start | bytes 2359300
Sparse Core Ops, SparseCore 0:
  31.1 38.0 reduce-scatter.2
  206.5 36.3 reduce-scatter.4
Sparse Core Ops, SparseCore 1:
  33.1 80.8 all-gather.2
  115.4 79.1 all-gather.4
